TPU v7x, 32 devices: a whole 2x2x4 slice. The times are simulated.
32 devices in a mesh: grp: 2 (over y), fs: 4 (over z), tp: 4 (over x, core).
Axes of the slice: x: 2, y: 2, z: 4, core: 2. Of those that a mesh axis runs over, the one named last changes fastest.
Arguments:
- tokens: bfloat16 [2048, 2048], P(('grp', 'fs')), parts along dimension 0, may hold values from -6 to 6
- norm_gain: float32 [2048], P('fs'), may hold values from 0.1 to 1.9
- gate_master: float32 [4, 2048, 1024], P(None, 'fs', 'tp'), may hold values from -0.125 to 0.125
- up_master: float32 [4, 2048, 1024], P(None, 'fs', 'tp'), may hold values from -0.125 to 0.125
- chosen: int32 [2048, 2], P(('grp', 'fs')), parts along dimension 0, may hold values from 0 to 3, all different within a row; in each aligned block of 256 rows (0 to 255, 256 to 511, ...) at most 256 rows name the same one
- affinity: float32 [2048, 2], P(('grp', 'fs')), parts along dimension 0, may hold values from 0.05 to 1
Outputs:
- gate_served: bfloat16 [8, 2048, 1024], P(('grp', 'fs'), None, 'tp'), parts along dimension 0
- up_served: bfloat16 [8, 2048, 1024], P(('grp', 'fs'), None, 'tp'), parts along dimension 0
- hidden: bfloat16 [2048, 2, 1024], P(('grp', 'fs'), None, 'tp'), parts along dimension 0
There are 2 independent parts, one for each index of `grp`. A program takes and returns all parts, laid end to end along the dimension named above; an argument that names none is the same for every part. Nothing has to cross between parts.
Inputs may be any that keep to these rules, and one draw needn't show every extreme that they name: Among the rows of one index of fs (256 tokens, all their choices) no expert is chosen more than 256 times, a bound that some block reaches; the choices of one token differ.
All inputs are finite; a program needn't handle non-finite values.
Results may differ from a plain program's by a relative error of at most 0.023.
Values may be sent and summed in bfloat16 or wider, within the bound.
A program may use at most 64 MiB of HBM per device.

v0:
```python
import jax
import jax.numpy as jnp
from jax import lax
from jax.sharding import PartitionSpec as P


def on_device(tokens, norm_gain, gate_master, up_master, chosen, affinity):
    folded_gate = (gate_master * norm_gain[None, :, None]).astype(jnp.bfloat16)
    folded_up = (up_master * norm_gain[None, :, None]).astype(jnp.bfloat16)
    new_gate, new_up = (
        lax.all_to_all(folded_gate, "fs", split_axis=0, concat_axis=1, tiled=True),
        lax.all_to_all(folded_up, "fs", split_axis=0, concat_axis=1, tiled=True),
    )
    experts_all = gate_master.shape[0]
    tok_rows, width = tokens.shape
    top = chosen.shape[1]
    capacity = tok_rows * top * 2 // experts_all
    local = new_gate.shape[0]
    xfloat = tokens.astype(jnp.float32)
    scale = lax.rsqrt(jnp.mean(xfloat * xfloat, axis=-1) + 1e-06)
    share = affinity / jnp.sum(affinity, axis=-1, keepdims=True)
    flat_e = chosen.reshape(-1)
    onehot = (flat_e[:, None] == jnp.arange(experts_all, dtype=jnp.int32)[None, :]).astype(
        jnp.int32
    )
    slot = jnp.sum((jnp.cumsum(onehot, axis=0) - onehot) * onehot, axis=1)
    target = flat_e * capacity + slot
    owner = jnp.repeat(jnp.arange(tok_rows, dtype=jnp.int32), top)
    total = experts_all * capacity
    scale_buf = (
        jnp.zeros((total,), jnp.float32).at[target].set(scale[owner]).reshape(experts_all, capacity)
    )
    share_buf = (
        jnp.zeros((total,), jnp.float32)
        .at[target]
        .set(share.reshape(-1))
        .reshape(experts_all, capacity)
    )
    narrow = width // lax.axis_size("tp")
    own_cols = lax.dynamic_slice_in_dim(tokens, lax.axis_index("tp") * narrow, narrow, 1)
    row_buf = jnp.zeros((total, narrow), jnp.bfloat16).at[target].set(own_cols[owner])
    row_buf = row_buf.reshape(experts_all, capacity, narrow)
    got_rows, got_scale, got_share = (
        lax.all_to_all(row_buf, "fs", split_axis=0, concat_axis=0, tiled=True),
        lax.all_to_all(
            scale_buf.astype(jnp.bfloat16), "fs", split_axis=0, concat_axis=0, tiled=True
        ).astype(scale_buf.dtype),
        lax.all_to_all(
            share_buf.astype(jnp.bfloat16), "fs", split_axis=0, concat_axis=0, tiled=True
        ).astype(share_buf.dtype),
    )
    sources = got_rows.shape[0] // local
    got_rows = got_rows.reshape(sources, local, capacity, narrow)
    piece = lax.all_gather(got_rows, "tp", axis=3, tiled=True)
    more_gate = jnp.einsum("secd,edf->secf", piece, new_gate, preferred_element_type=jnp.float32)
    more_up = jnp.einsum("secd,edf->secf", piece, new_up, preferred_element_type=jnp.float32)
    gate = more_gate
    up = more_up
    factor = got_scale.reshape(sources, local, capacity)[..., None]
    weight = got_share.reshape(sources, local, capacity)[..., None]
    gate = gate * factor
    up = up * factor
    hidden_rows = (weight * jax.nn.silu(gate) * up).astype(jnp.bfloat16)
    hidden_rows = hidden_rows.reshape(sources * local, capacity, hidden_rows.shape[3])
    back = lax.all_to_all(hidden_rows, "fs", split_axis=0, concat_axis=0, tiled=True)
    picked = back.reshape(total, back.shape[2])[target].reshape(tok_rows, top, back.shape[2])
    return (new_gate, new_up, picked)


def solution(mesh):
    return jax.shard_map(
        on_device,
        mesh=mesh,
        in_specs=(
            P(("grp", "fs"), None),
            P("fs"),
            P(None, "fs", "tp"),
            P(None, "fs", "tp"),
            P(("grp", "fs"), None),
            P(("grp", "fs"), None),
        ),
        out_specs=(
            P(("grp", "fs"), None, "tp"),
            P(("grp", "fs"), None, "tp"),
            P(("grp", "fs"), None, "tp"),
        ),
        check_vma=False,
    )
```

profile of v0, /device:TPU:0, one launch (start us, length us, event | category | flops | bytes accessed | tf_op | source)
XLA Modules:
  0.0 163.8 jit_solution(18356809726918053598)
XLA Ops:
  7.2 0.0 all-gather.3.cloned.1.call-start
  7.2 0.7 broadcast_multiply_fusion
  7.9 0.8 copy.26
  8.7 0.1 eq.29
  8.9 0.1 eq.25
  9.0 0.1 copy.25
  9.1 0.1 mul.75
  9.3 1.2 reduce-window.6
  10.5 0.2 slice_reduce_fusion
  10.8 0.2 reduce-window.9
  10.9 0.1 add_bitcast_fusion
  11.0 0.1 reshape.174
  11.2 1.0 constant_dynamic-slice_fusion
  12.2 0.0 copy-start.1
  12.2 0.0 copy-start
  12.2 5.0 %scatter_custom_fusion.1 = bf16[1024,512]{1,0:T(8,128)(2,1)S(1)} fusion(s32[512]{0:T(512)S(1)} %bitcast.83, bf16[256,512]{1,0:T(8,128)(2,1)S(1)} %constant_dynamic-slice_fusion, s32[1024]{0:T(1024)S(1)} %pad_clamp_fusion.1, bf16[]{:T(256)} %constant.15.clone.1), kind=kCustom, calls=%fused_computation.18 | custom fusion | bytes 1048578 | tf_op jit(solution)/shard_map/scatter | solution.py:41
  17.3 32.0 %all_to_all.46 = bf16[4,256,512]{2,1,0:T(8,128)(2,1)} all-to-all(bf16[4,256,512]{2,1,0:T(8,128)(2,1)S(1)} %bitcast.82), channel_id=1, replica_groups=mesh['grp'=2,'fs'=4,'tp'=4] {'fs'}, dimensions={0} | all-to-all | bytes 2097152 | tf_op jit(solution)/shard_map/all_to_all | solution.py:44
  49.3 0.0 all-gather.3.cloned.1.call-update
  49.3 0.0 copy-done.1
  49.3 0.1 copy.28
  49.5 0.1 reshape.212
  49.6 2.4 %scatter_custom_fusion = f32[1024]{0:T(1024)S(1)} fusion(s32[512]{0:T(512)S(1)} %bitcast.84, f32[512]{0:T(512)S(1)} %reshape.212, f32[]{:T(128)} %constant.11.clone.1), kind=kCustom, calls=%fused_computation.38 | custom fusion | bytes 4100 | tf_op jit(solution)/shard_map/scatter | solution.py:36
  52.1 0.5 broadcast.103
  52.6 0.7 reduce.3
  53.3 0.6 reshape.249
  53.9 3.2 %all-to-all-start.2 = ((bf16[4,2,128]{2,1,0:T(2,128)(2,1)}), bf16[4,2,128]{2,1,0:T(2,128)(2,1)S(1)}, u32[]{:S(2)}, u32[]{:S(2)}) async-start(bf16[4,2,128]{2,1,0:T(2,128)(2,1)} %reshape.249), calls=%async_computation.2 | async-start | bytes 4096 | tf_op jit(solution)/shard_map/all_to_all | solution.py:48
  57.1 0.3 multiply_reduce_fusion
  57.4 3.5 %gather_fusion = f32[512]{0:T(512)S(1)} fusion(f32[256]{0:T(256)S(1)} %add_rsqrt_fusion, s32[1024]{0:T(1024)S(1)} %pad_clamp_fusion.1), kind=kCustom, calls=%fused_computation.1 | custom fusion | bytes 6144 | tf_op jit(solution)/shard_map/gather | solution.py:31
  61.0 2.4 %scatter_custom_fusion.2 = f32[1024]{0:T(1024)S(1)} fusion(s32[512]{0:T(512)S(1)} %bitcast.85, f32[512]{0:T(512)S(1)} %gather_fusion, f32[]{:T(128)} %constant.11.clone.1), kind=kCustom, calls=%fused_computation.36 | custom fusion | bytes 4100 | tf_op jit(solution)/shard_map/scatter | solution.py:31
  63.4 0.7 reduce.2
  64.1 0.6 reshape.247
  64.7 0.0 all-to-all-done.2
  64.7 5.0 %all-to-all-start.4 = ((bf16[4,2,128]{2,1,0:T(2,128)(2,1)}), bf16[4,2,128]{2,1,0:T(2,128)(2,1)S(1)}, u32[]{:S(2)}, u32[]{:S(2)}) async-start(bf16[4,2,128]{2,1,0:T(2,128)(2,1)} %reshape.247), calls=%async_computation.4 | async-start | bytes 4096 | tf_op jit(solution)/shard_map/all_to_all | solution.py:45
  69.7 3.5 %multiply_convert_fusion = (bf16[4,512,256]{2,1,0:T(8,128)(2,1)}, bf16[4,512,256]{2,1,0:T(8,128)(2,1)S(1)}) fusion(f32[4,512,256]{2,1,0:T(8,128)} %param.9, f32[512]{0:T(512)S(1)} %copy-done.2, f32[4,512,256]{2,1,0:T(8,128)} %param.8), kind=kLoop, calls=%fused_computation.7 | loop fusion | flops 2097152 | bytes 6293504 | tf_op jit(solution)/shard_map/convert_element_type | solution.py:9
  73.3 2.0 %all-to-all-done.4 = bf16[4,2,128]{2,1,0:T(2,128)(2,1)S(1)} async-done(((bf16[4,2,128]{2,1,0:T(2,128)(2,1)}), bf16[4,2,128]{2,1,0:T(2,128)(2,1)S(1)}, u32[]{:S(2)}, u32[]{:S(2)}) %all-to-all-start.4) | async-done | bytes 2080 | tf_op jit(solution)/shard_map/all_to_all | solution.py:45
  75.2 26.7 %all_to_all.47 = bf16[4,512,256]{2,1,0:T(8,128)(2,1)S(1)} all-to-all(bf16[4,512,256]{2,1,0:T(8,128)(2,1)S(1)} %get-tuple-element.4), channel_id=1, replica_groups=mesh['grp'=2,'fs'=4,'tp'=4] {'fs'}, dimensions={0} | all-to-all | bytes 2097152 | tf_op jit(solution)/shard_map/all_to_all | solution.py:11
  101.9 3.7 %all-to-all-start.1 = ((bf16[4,512,256]{2,1,0:T(8,128)(2,1)}), bf16[4,512,256]{2,1,0:T(8,128)(2,1)S(1)}, u32[]{:S(2)}, u32[]{:S(2)}) async-start(bf16[4,512,256]{2,1,0:T(8,128)(2,1)} %get-tuple-element.3), calls=%async_computation.1 | async-start | bytes 2097152 | tf_op jit(solution)/shard_map/all_to_all | solution.py:12
  105.7 0.0 all-gather.3.cloned.1.call-done
  105.7 3.5 %fusion.3 = f32[4,1,256,256]{2,3,0,1:T(8,128)S(1)} fusion(bf16[2048,256,1]{1,0,2:T(8,128)(2,1)S(1)} %bitcast.78, bf16[4,256,2048]{2,1,0:T(8,128)(2,1)} %all-gather.3.cloned.1.call-done, f32[4,256]{1,0:T(4,128)S(1)} %bitcast.91), kind=kOutput, calls=%fused_computation.14 | convolution fusion | flops 1074003968 | bytes 6295552 | tf_op jit(solution)/shard_map/secd,edf->secf/dot_general | solution.py:55
  109.2 20.8 %all-to-all-done.1 = bf16[4,512,256]{2,1,0:T(8,128)(2,1)S(1)} async-done(((bf16[4,512,256]{2,1,0:T(8,128)(2,1)}), bf16[4,512,256]{2,1,0:T(8,128)(2,1)S(1)}, u32[]{:S(2)}, u32[]{:S(2)}) %all-to-all-start.1) | async-done | bytes 1048608 | tf_op jit(solution)/shard_map/all_to_all | solution.py:12
  130.1 4.5 %fusion.6 = bf16[4,256,256]{1,2,0:T(8,128)(2,1)} fusion(bf16[2048,256,1]{1,0,2:T(8,128)(2,1)S(1)} %bitcast.80, bf16[4,256,2048]{2,1,0:T(8,128)(2,1)} %all-gather.3.cloned.1.call-done, f32[4,1,256,256]{2,3,0,1:T(8,128)S(1)} %fusion.3, f32[4,256]{1,0:T(4,128)S(1)} %bitcast.92, f32[4,256]{1,0:T(4,128)S(1)} %bitcast.90), kind=kOutput, calls=%fused_computation.17 | convolution fusion | flops 1075838976 | bytes 6823936 | tf_op jit(solution)/shard_map/secd,edf->secf/dot_general | solution.py:56
  134.6 3.5 %all-to-all-start.5 = ((bf16[4,256,256]{1,2,0:T(8,128)(2,1)}), bf16[4,256,256]{1,2,0:T(8,128)(2,1)S(1)}, u32[]{:S(2)}, u32[]{:S(2)}) async-start(bf16[4,256,256]{1,2,0:T(8,128)(2,1)} %fusion.6), calls=%async_computation.5 | async-start | bytes 1048576 | tf_op jit(solution)/shard_map/all_to_all | solution.py:65
  138.1 14.0 %all-to-all-done.5 = bf16[4,256,256]{1,2,0:T(8,128)(2,1)S(1)} async-done(((bf16[4,256,256]{1,2,0:T(8,128)(2,1)}), bf16[4,256,256]{1,2,0:T(8,128)(2,1)S(1)}, u32[]{:S(2)}, u32[]{:S(2)}) %all-to-all-start.5) | async-done | bytes 524320 | tf_op jit(solution)/shard_map/all_to_all | solution.py:65
  152.1 0.2 copy.33
  152.3 2.0 %gather_fusion.1 = bf16[512,256]{1,0:T(8,128)(2,1)S(1)} fusion(bf16[1024,256]{1,0:T(8,128)(2,1)S(1)} %bitcast.77, s32[1024]{0:T(1024)S(1)} %pad_clamp_fusion), kind=kCustom, calls=%fused_computation.2 | custom fusion | bytes 526336 | tf_op jit(solution)/shard_map/gather | solution.py:66
  154.2 0.8 reshape.181
  155.0 1.0 copy.46
  156.0 1.0 copy.47
  (21 shorter events, 0.2 us)
Async XLA Ops:
  7.2 98.6 %all-gather.3.cloned.1.call-start = ((), (), s32[]{:S(2)}) async-start(), calls=%async_computation.6 | async-start | bytes 5242880 | tf_op jit(solution)/shard_map/all_gather | solution.py:54
  12.2 37.1 %copy-start.1 = (f32[256,2]{0,1:T(2,128)S(1)}, f32[256,2]{0,1:T(2,128)}, u32[]{:S(2)}) copy-start(f32[256,2]{0,1:T(2,128)} %param.11) | copy-start | bytes 6148
  12.2 44.9 %copy-start = (bf16[256,2048]{1,0:T(8,128)(2,1)S(1)}, bf16[256,2048]{1,0:T(8,128)(2,1)}, u32[]{:S(2)}) copy-start(bf16[256,2048]{1,0:T(8,128)(2,1)} %param.6) | copy-start | bytes 3145732
  49.3 20.5 %copy-start.2 = (f32[512]{0:T(512)S(1)}, f32[512]{0:T(512)}, u32[]{:S(2)}) copy-start(f32[512]{0:T(512)} %param.7) | copy-start | bytes 6148
  53.9 10.8 %all-to-all-start.2 = ((bf16[4,2,128]{2,1,0:T(2,128)(2,1)}), bf16[4,2,128]{2,1,0:T(2,128)(2,1)S(1)}, u32[]{:S(2)}, u32[]{:S(2)}) async-start(bf16[4,2,128]{2,1,0:T(2,128)(2,1)} %reshape.249), calls=%async_computation.2 | async-start | bytes 4096 | tf_op jit(solution)/shard_map/all_to_all | solution.py:48
  64.7 10.5 %all-to-all-start.4 = ((bf16[4,2,128]{2,1,0:T(2,128)(2,1)}), bf16[4,2,128]{2,1,0:T(2,128)(2,1)S(1)}, u32[]{:S(2)}, u32[]{:S(2)}) async-start(bf16[4,2,128]{2,1,0:T(2,128)(2,1)} %reshape.247), calls=%async_computation.4 | async-start | bytes 4096 | tf_op jit(solution)/shard_map/all_to_all | solution.py:45
  101.9 28.1 %all-to-all-start.1 = ((bf16[4,512,256]{2,1,0:T(8,128)(2,1)}), bf16[4,512,256]{2,1,0:T(8,128)(2,1)S(1)}, u32[]{:S(2)}, u32[]{:S(2)}) async-start(bf16[4,512,256]{2,1,0:T(8,128)(2,1)} %get-tuple-element.3), calls=%async_computation.1 | async-start | bytes 2097152 | tf_op jit(solution)/shard_map/all_to_all | solution.py:12
  134.6 17.5 %all-to-all-start.5 = ((bf16[4,256,256]{1,2,0:T(8,128)(2,1)}), bf16[4,256,256]{1,2,0:T(8,128)(2,1)S(1)}, u32[]{:S(2)}, u32[]{:S(2)}) async-start(bf16[4,256,256]{1,2,0:T(8,128)(2,1)} %fusion.6), calls=%async_computation.5 | async-start | bytes 1048576 | tf_op jit(solution)/shard_map/all_to_all | solution.py:65
Sparse Core Ops, SparseCore 0:
  49.4 33.5 all-gather.2
where the time goes:
time: 164 us
  blocking collectives  58.7 us (36%)
  waiting for transfers between devices  36.8 us (22%)
  local copies, waits for them, and re-layouts  23.1 us (14%)
  starting transfers between devices  15.5 us (9%)
  between operations  14.3 us (9%)
  matrix products  7.99 us (5%)
  other arithmetic  7.42 us (5%)
    all_to_all x1, blocking collectives, on_device(): lax.all_to_all(row_buf, 'fs', split_axis=0, concat_axis=0, tiled=True)  32 us
    all_to_all x1, blocking collectives, on_device(): lax.all_to_all(folded_gate, 'fs', split_axis=0, concat_axis=1, tiled=True)  26.7 us
    all_to_all x1, waiting for transfers between devices, on_device(): lax.all_to_all(folded_up, 'fs', split_axis=0, concat_axis=1, tiled=True)  20.8 us
    all_to_all x1, waiting for transfers between devices, on_device(): lax.all_to_all(hidden_rows, 'fs', split_axis=0, concat_axis=0, tiled=True)  14 us
    all_to_all x1, starting transfers between devices, on_device(): lax.all_to_all(scale_buf.astype(jnp.bfloat16), 'fs', split_axis=0, concat...  5.05 us
    scatter x1, local copies, waits for them, and re-layouts, on_device(): jnp.zeros((total, narrow), jnp.bfloat16).at[target].set(own_cols[owner])  5.05 us
    dot_general x1, matrix products, on_device(): jnp.einsum('secd,edf->secf', piece, new_up, preferred_element_type=jnp.fl...  4.48 us
    unnamed x15, local copies, waits for them, and re-layouts  3.97 us
  transfers between devices with their start and end apart: 5, of which 3 were waited for; matrix products, arithmetic and copies ran while one was open for 12% of the time, Pallas kernels for 0%

commit v1 on v0

--- a/solution.py
+++ b/solution.py
@@ -1,7 +1,35 @@
+import functools
 import jax
 import jax.numpy as jnp
 from jax import lax
 from jax.sharding import PartitionSpec as P
+
+
+def update_stacks_all(my_data, where_dim, arr):
+    new, spare = (my_data.shape[:where_dim], my_data.shape[where_dim + 1 :])
+    return jnp.moveaxis(my_data.reshape(*new, arr, -1, *spare), where_dim, 0)
+
+
+def pack_numbers_up(array_here, row_dim):
+    state_next = list(array_here.shape[1:])
+    state_next[row_dim] *= array_here.shape[0]
+    return jnp.moveaxis(array_here, 0, row_dim).reshape(state_next)
+
+
+def define_fields_up(vec, axis_tag, shard_in, piece_in):
+    left_arr, block_next = (lax.axis_size(axis_tag), lax.axis_index(axis_tag))
+    val = update_stacks_all(vec, shard_in, left_arr)
+    fields = [val[block_next]]
+    for i0 in range(1, left_arr):
+        y = val[(block_next + i0) % left_arr]
+        fields.append(
+            lax.ppermute(y, axis_tag, [(dd, (dd + i0) % left_arr) for dd in range(left_arr)])
+        )
+    val = jnp.stack(fields)[(block_next - jnp.arange(left_arr)) % left_arr]
+    return pack_numbers_up(val, piece_in)
+
+
+_pass_stages_all = functools.partial(define_fields_up, axis_tag="fs", shard_in=0, piece_in=0)
 
 
 def on_device(tokens, norm_gain, gate_master, up_master, chosen, affinity):
@@ -41,7 +69,7 @@
     row_buf = jnp.zeros((total, narrow), jnp.bfloat16).at[target].set(own_cols[owner])
     row_buf = row_buf.reshape(experts_all, capacity, narrow)
     got_rows, got_scale, got_share = (
-        lax.all_to_all(row_buf, "fs", split_axis=0, concat_axis=0, tiled=True),
+        _pass_stages_all(row_buf),
         lax.all_to_all(
             scale_buf.astype(jnp.bfloat16), "fs", split_axis=0, concat_axis=0, tiled=True
         ).astype(scale_buf.dtype),

time: 164 us -> 163 us (level)
  blocking collectives: 58.7 us -> 26.9 us
  waiting for transfers between devices: 36.8 us -> 58.2 us
  starting transfers between devices: 15.5 us -> 22.5 us
  local copies, waits for them, and re-layouts: 23.1 us -> 24.8 us
    all_to_all x1 -> x0, blocking collectives: 32 us -> none  [on_device(): lax.all_to_all(row_buf, 'fs', split_axis=0, concat_axis=0, tiled=True)]
    ppermute x0 -> x3, waiting for transfers between devices: none -> 21.3 us  [define_fields_up(): lax.ppermute(y, axis_tag, [(dd, (dd + i0) % left_arr) for dd in range(lef...]
    ppermute x0 -> x3, starting transfers between devices: none -> 6.14 us  [define_fields_up(): lax.ppermute(y, axis_tag, [(dd, (dd + i0) % left_arr) for dd in range(lef...]
  transfers between devices with their start and end apart: 5 -> 8, of which waited for: 3 -> 5; matrix products, arithmetic and copies ran while one was open for 12% -> 12% of each run, Pallas kernels for 0% -> 0%
where the time goes in v1:
time: 163 us; the launch traced here: 162 us
  waiting for transfers between devices  58.2 us (36%)
  blocking collectives  26.9 us (17%)
  local copies, waits for them, and re-layouts  24.8 us (15%)
  starting transfers between devices  22.5 us (14%)
  between operations  14.3 us (9%)
  matrix products  8.01 us (5%)
  other arithmetic  7.53 us (5%)
    all_to_all x1, blocking collectives, on_device(): lax.all_to_all(folded_gate, 'fs', split_axis=0, concat_axis=1, tiled=True)  26.9 us
    ppermute x3, waiting for transfers between devices, define_fields_up(): lax.ppermute(y, axis_tag, [(dd, (dd + i0) % left_arr) for dd in range(lef...  21.3 us
    all_to_all x1, waiting for transfers between devices, on_device(): lax.all_to_all(folded_up, 'fs', split_axis=0, concat_axis=1, tiled=True)  20.9 us
    all_to_all x1, waiting for transfers between devices, on_device(): lax.all_to_all(hidden_rows, 'fs', split_axis=0, concat_axis=0, tiled=True)  14 us
    ppermute x3, starting transfers between devices, define_fields_up(): lax.ppermute(y, axis_tag, [(dd, (dd + i0) % left_arr) for dd in range(lef...  6.14 us
    all_to_all x1, starting transfers between devices, on_device(): lax.all_to_all(scale_buf.astype(jnp.bfloat16), 'fs', split_axis=0, concat...  5.09 us
    scatter x1, local copies, waits for them, and re-layouts, on_device(): jnp.zeros((total, narrow), jnp.bfloat16).at[target].set(own_cols[owner])  5.05 us
    dot_general x1, matrix products, on_device(): jnp.einsum('secd,edf->secf', piece, new_up, preferred_element_type=jnp.fl...  4.49 us
  transfers between devices with their start and end apart: 8, of which 5 were waited for; matrix products, arithmetic and copies ran while one was open for 12% of the time, Pallas kernels for 0%

profile of v1, /device:TPU:0, one launch (start us, length us, event | category | flops | bytes accessed | tf_op | source)
XLA Modules:
  0.0 162.3 jit_solution(3044028011890907987)
XLA Ops:
  7.2 0.0 all-gather.3.cloned.1.call-start
  7.3 0.7 broadcast_multiply_fusion
  7.9 0.8 copy.26
  8.8 0.1 eq.35
  8.9 0.1 eq.31
  9.0 0.1 copy.25
  9.2 0.1 mul.75
  9.3 1.2 reduce-window.6
  10.6 0.2 slice_reduce_fusion
  10.8 0.2 reduce-window.9
  11.0 0.1 add_bitcast_fusion
  11.1 0.1 reshape.217
  11.3 1.0 constant_dynamic-slice_fusion.1
  12.3 5.0 %scatter_custom_fusion.1 = bf16[1024,512]{1,0:T(8,128)(2,1)S(1)} fusion(s32[512]{0:T(512)S(1)} %bitcast.99, bf16[256,512]{1,0:T(8,128)(2,1)S(1)} %constant_dynamic-slice_fusion.1, s32[1024]{0:T(1024)S(1)} %pad_clamp_fusion.2, bf16[]{:T(256)} %constant.58.clone.1), kind=kCustom, calls=%fused_computation.20 | custom fusion | bytes 1048578 | tf_op jit(solution)/shard_map/scatter | solution.py:69
  17.3 0.1 constant_dynamic-slice_fusion
  17.4 5.1 %collective-permute-start.2 = (bf16[1,256,512]{2,1,0:T(8,128)(2,1)S(1)}, bf16[1,256,512]{2,1,0:T(8,128)(2,1)S(1)}, u32[]{:S(2)}, u32[]{:S(2)}) collective-permute-start(bf16[1,256,512]{2,1,0:T(8,128)(2,1)S(1)} %get-tuple-element.4), channel_id=1, source_target_pairs={{0,12},{4,0},{8,4},{12,8},{1,13},{5,1},{9,5},{13,9},{2,14},{6,2},{... | collective-permute-start | bytes 786440 | tf_op jit(solution)/shard_map/ppermute | solution.py:26
  22.6 1.0 collective-permute-start
  23.6 5.7 %collective-permute-done.2 = bf16[1,256,512]{2,1,0:T(8,128)(2,1)S(1)} collective-permute-done((bf16[1,256,512]{2,1,0:T(8,128)(2,1)S(1)}, bf16[1,256,512]{2,1,0:T(8,128)(2,1)S(1)}, u32[]{:S(2)}, u32[]{:S(2)}) %collective-permute-start.2) | collective-permute-done | bytes 262176 | tf_op jit(solution)/shard_map/ppermute | solution.py:26
  29.3 15.6 %collective-permute-done.1 = bf16[1,256,512]{2,1,0:T(8,128)(2,1)S(1)} collective-permute-done((bf16[1,256,512]{2,1,0:T(8,128)(2,1)S(1)}, bf16[1,256,512]{2,1,0:T(8,128)(2,1)S(1)}, u32[]{:S(2)}, u32[]{:S(2)}) %collective-permute-start.1) | collective-permute-done | bytes 262176 | tf_op jit(solution)/shard_map/ppermute | solution.py:26
  44.9 0.1 maximum_bitcast_fusion
  45.0 1.6 gather_fusion
  46.7 0.1 copy.28
  46.8 0.1 reshape.263
  47.0 2.4 %scatter_custom_fusion = f32[1024]{0:T(1024)S(1)} fusion(s32[512]{0:T(512)S(1)} %bitcast.100, f32[512]{0:T(512)S(1)} %reshape.263, f32[]{:T(128)} %constant.54.clone.1), kind=kCustom, calls=%fused_computation.47 | custom fusion | bytes 4100 | tf_op jit(solution)/shard_map/scatter | solution.py:64
  49.5 0.5 broadcast.175
  50.0 0.7 reduce.3
  50.6 0.6 reshape.300
  51.2 4.1 %all-to-all-start.2 = ((bf16[4,2,128]{2,1,0:T(2,128)(2,1)}), bf16[4,2,128]{2,1,0:T(2,128)(2,1)S(1)}, u32[]{:S(2)}, u32[]{:S(2)}) async-start(bf16[4,2,128]{2,1,0:T(2,128)(2,1)} %reshape.300), calls=%async_computation.2 | async-start | bytes 4096 | tf_op jit(solution)/shard_map/all_to_all | solution.py:76
  55.3 0.3 multiply_reduce_fusion
  55.6 3.5 %gather_fusion.1 = f32[512]{0:T(512)S(1)} fusion(f32[256]{0:T(256)S(1)} %add_rsqrt_fusion, s32[1024]{0:T(1024)S(1)} %pad_clamp_fusion.2), kind=kCustom, calls=%fused_computation.2 | custom fusion | bytes 6144 | tf_op jit(solution)/shard_map/gather | solution.py:59
  59.1 2.4 %scatter_custom_fusion.2 = f32[1024]{0:T(1024)S(1)} fusion(s32[512]{0:T(512)S(1)} %bitcast.101, f32[512]{0:T(512)S(1)} %gather_fusion.1, f32[]{:T(128)} %constant.54.clone.1), kind=kCustom, calls=%fused_computation.45 | custom fusion | bytes 4100 | tf_op jit(solution)/shard_map/scatter | solution.py:59
  61.6 0.7 reduce.2
  62.3 0.6 reshape.298
  62.8 5.1 %all-to-all-start.3 = ((bf16[4,2,128]{2,1,0:T(2,128)(2,1)}), bf16[4,2,128]{2,1,0:T(2,128)(2,1)S(1)}, u32[]{:S(2)}, u32[]{:S(2)}) async-start(bf16[4,2,128]{2,1,0:T(2,128)(2,1)} %reshape.298), calls=%async_computation.3 | async-start | bytes 4096 | tf_op jit(solution)/shard_map/all_to_all | solution.py:73
  67.9 3.5 %multiply_convert_fusion = (bf16[4,512,256]{2,1,0:T(8,128)(2,1)}, bf16[4,512,256]{2,1,0:T(8,128)(2,1)S(1)}) fusion(f32[4,512,256]{2,1,0:T(8,128)} %param.9, f32[512]{0:T(512)S(1)} %copy-done.2, f32[4,512,256]{2,1,0:T(8,128)} %param.8), kind=kLoop, calls=%fused_computation.8 | loop fusion | flops 2097152 | bytes 6293504 | tf_op jit(solution)/shard_map/convert_element_type | solution.py:37
  71.4 2.0 %all-to-all-done.3 = bf16[4,2,128]{2,1,0:T(2,128)(2,1)S(1)} async-done(((bf16[4,2,128]{2,1,0:T(2,128)(2,1)}), bf16[4,2,128]{2,1,0:T(2,128)(2,1)S(1)}, u32[]{:S(2)}, u32[]{:S(2)}) %all-to-all-start.3) | async-done | bytes 2080 | tf_op jit(solution)/shard_map/all_to_all | solution.py:73
  73.4 26.9 %all_to_all.41 = bf16[4,512,256]{2,1,0:T(8,128)(2,1)S(1)} all-to-all(bf16[4,512,256]{2,1,0:T(8,128)(2,1)S(1)} %get-tuple-element.8), channel_id=1, replica_groups=mesh['grp'=2,'fs'=4,'tp'=4] {'fs'}, dimensions={0} | all-to-all | bytes 2097152 | tf_op jit(solution)/shard_map/all_to_all | solution.py:39
  100.4 3.7 %all-to-all-start.1 = ((bf16[4,512,256]{2,1,0:T(8,128)(2,1)}), bf16[4,512,256]{2,1,0:T(8,128)(2,1)S(1)}, u32[]{:S(2)}, u32[]{:S(2)}) async-start(bf16[4,512,256]{2,1,0:T(8,128)(2,1)} %get-tuple-element.7), calls=%async_computation.1 | async-start | bytes 2097152 | tf_op jit(solution)/shard_map/all_to_all | solution.py:40
  104.2 3.5 %fusion.3 = f32[4,1,256,256]{2,3,0,1:T(8,128)S(1)} fusion(bf16[2048,256,1]{1,0,2:T(8,128)(2,1)S(1)} %bitcast.92, bf16[4,256,2048]{2,1,0:T(8,128)(2,1)} %all-gather.3.cloned.1.call-done, f32[4,256]{1,0:T(4,128)S(1)} %bitcast.107), kind=kOutput, calls=%fused_computation.15 | convolution fusion | flops 1074003968 | bytes 6295552 | tf_op jit(solution)/shard_map/secd,edf->secf/dot_general | solution.py:83
  107.7 20.9 %all-to-all-done.1 = bf16[4,512,256]{2,1,0:T(8,128)(2,1)S(1)} async-done(((bf16[4,512,256]{2,1,0:T(8,128)(2,1)}), bf16[4,512,256]{2,1,0:T(8,128)(2,1)S(1)}, u32[]{:S(2)}, u32[]{:S(2)}) %all-to-all-start.1) | async-done | bytes 1048608 | tf_op jit(solution)/shard_map/all_to_all | solution.py:40
  128.6 4.5 %fusion.6 = bf16[4,256,256]{1,2,0:T(8,128)(2,1)} fusion(bf16[2048,256,1]{1,0,2:T(8,128)(2,1)S(1)} %bitcast.94, bf16[4,256,2048]{2,1,0:T(8,128)(2,1)} %all-gather.3.cloned.1.call-done, f32[4,1,256,256]{2,3,0,1:T(8,128)S(1)} %fusion.3, f32[4,256]{1,0:T(4,128)S(1)} %bitcast.108, f32[4,256]{1,0:T(4,128)S(1)} %bitcast.106), kind=kOutput, calls=%fused_computation.18 | convolution fusion | flops 1075838976 | bytes 6823936 | tf_op jit(solution)/shard_map/secd,edf->secf/dot_general | solution.py:84
  133.0 3.5 %all-to-all-start.4 = ((bf16[4,256,256]{1,2,0:T(8,128)(2,1)}), bf16[4,256,256]{1,2,0:T(8,128)(2,1)S(1)}, u32[]{:S(2)}, u32[]{:S(2)}) async-start(bf16[4,256,256]{1,2,0:T(8,128)(2,1)} %fusion.6), calls=%async_computation.4 | async-start | bytes 1048576 | tf_op jit(solution)/shard_map/all_to_all | solution.py:93
  136.5 14.0 %all-to-all-done.4 = bf16[4,256,256]{1,2,0:T(8,128)(2,1)S(1)} async-done(((bf16[4,256,256]{1,2,0:T(8,128)(2,1)}), bf16[4,256,256]{1,2,0:T(8,128)(2,1)S(1)}, u32[]{:S(2)}, u32[]{:S(2)}) %all-to-all-start.4) | async-done | bytes 524320 | tf_op jit(solution)/shard_map/all_to_all | solution.py:93
  150.5 0.2 copy.33
  150.7 2.0 %gather_fusion.2 = bf16[512,256]{1,0:T(8,128)(2,1)S(1)} fusion(bf16[1024,256]{1,0:T(8,128)(2,1)S(1)} %bitcast.90, s32[1024]{0:T(1024)S(1)} %pad_clamp_fusion), kind=kCustom, calls=%fused_computation.3 | custom fusion | bytes 526336 | tf_op jit(solution)/shard_map/gather | solution.py:94
  152.7 0.8 reshape.222
  153.5 1.0 copy.46
  154.5 1.0 copy.47
  (30 shorter events, 0.2 us)
Async XLA Ops:
  7.2 97.0 %all-gather.3.cloned.1.call-start = ((), (), s32[]{:S(2)}) async-start(), calls=%async_computation.5 | async-start | bytes 5242880 | tf_op jit(solution)/shard_map/all_gather | solution.py:82
  17.4 11.9 %collective-permute-start.2 = (bf16[1,256,512]{2,1,0:T(8,128)(2,1)S(1)}, bf16[1,256,512]{2,1,0:T(8,128)(2,1)S(1)}, u32[]{:S(2)}, u32[]{:S(2)}) collective-permute-start(bf16[1,256,512]{2,1,0:T(8,128)(2,1)S(1)} %get-tuple-element.4), channel_id=1, source_target_pairs={{0,12},{4,0},{8,4},{12,8},{1,13},{5,1},{9,5},{13,9},{2,14},{6,2},{... | collective-permute-start | bytes 786440 | tf_op jit(solution)/shard_map/ppermute | solution.py:26
  22.6 22.3 %collective-permute-start.1 = (bf16[1,256,512]{2,1,0:T(8,128)(2,1)S(1)}, bf16[1,256,512]{2,1,0:T(8,128)(2,1)S(1)}, u32[]{:S(2)}, u32[]{:S(2)}) collective-permute-start(bf16[1,256,512]{2,1,0:T(8,128)(2,1)S(1)} %get-tuple-element.5), channel_id=1, source_target_pairs={{0,8},{4,12},{8,0},{12,4},{1,9},{5,13},{9,1},{13,5},{2,10},{6,14},... | collective-permute-start | bytes 786440 | tf_op jit(solution)/shard_map/ppermute | solution.py:26
  22.6 22.3 %collective-permute-start = (bf16[1,256,512]{2,1,0:T(8,128)(2,1)S(1)}, bf16[1,256,512]{2,1,0:T(8,128)(2,1)S(1)}, u32[]{:S(2)}, u32[]{:S(2)}) collective-permute-start(bf16[1,256,512]{2,1,0:T(8,128)(2,1)S(1)} %get-tuple-element.6), channel_id=1, source_target_pairs={{0,4},{4,8},{8,12},{12,0},{1,5},{5,9},{9,13},{13,1},{2,6},{6,10},{... | collective-permute-start | bytes 786440 | tf_op jit(solution)/shard_map/ppermute | solution.py:26
  45.0 1.6 %copy-start.1 = (f32[256,2]{0,1:T(2,128)S(1)}, f32[256,2]{0,1:T(2,128)}, u32[]{:S(2)}) copy-start(f32[256,2]{0,1:T(2,128)} %param.11) | copy-start | bytes 6148
  45.0 10.3 %copy-start = (bf16[256,2048]{1,0:T(8,128)(2,1)S(1)}, bf16[256,2048]{1,0:T(8,128)(2,1)}, u32[]{:S(2)}) copy-start(bf16[256,2048]{1,0:T(8,128)(2,1)} %param.6) | copy-start | bytes 3145732
  46.6 21.3 %copy-start.2 = (f32[512]{0:T(512)S(1)}, f32[512]{0:T(512)}, u32[]{:S(2)}) copy-start(f32[512]{0:T(512)} %param.7) | copy-start | bytes 6148
  51.2 11.6 %all-to-all-start.2 = ((bf16[4,2,128]{2,1,0:T(2,128)(2,1)}), bf16[4,2,128]{2,1,0:T(2,128)(2,1)S(1)}, u32[]{:S(2)}, u32[]{:S(2)}) async-start(bf16[4,2,128]{2,1,0:T(2,128)(2,1)} %reshape.300), calls=%async_computation.2 | async-start | bytes 4096 | tf_op jit(solution)/shard_map/all_to_all | solution.py:76
  62.8 10.6 %all-to-all-start.3 = ((bf16[4,2,128]{2,1,0:T(2,128)(2,1)}), bf16[4,2,128]{2,1,0:T(2,128)(2,1)S(1)}, u32[]{:S(2)}, u32[]{:S(2)}) async-start(bf16[4,2,128]{2,1,0:T(2,128)(2,1)} %reshape.298), calls=%async_computation.3 | async-start | bytes 4096 | tf_op jit(solution)/shard_map/all_to_all | solution.py:73
  100.4 28.2 %all-to-all-start.1 = ((bf16[4,512,256]{2,1,0:T(8,128)(2,1)}), bf16[4,512,256]{2,1,0:T(8,128)(2,1)S(1)}, u32[]{:S(2)}, u32[]{:S(2)}) async-start(bf16[4,512,256]{2,1,0:T(8,128)(2,1)} %get-tuple-element.7), calls=%async_computation.1 | async-start | bytes 2097152 | tf_op jit(solution)/shard_map/all_to_all | solution.py:40
  133.0 17.5 %all-to-all-start.4 = ((bf16[4,256,256]{1,2,0:T(8,128)(2,1)}), bf16[4,256,256]{1,2,0:T(8,128)(2,1)S(1)}, u32[]{:S(2)}, u32[]{:S(2)}) async-start(bf16[4,256,256]{1,2,0:T(8,128)(2,1)} %fusion.6), calls=%async_computation.4 | async-start | bytes 1048576 | tf_op jit(solution)/shard_map/all_to_all | solution.py:93
Sparse Core Ops, SparseCore 0:
  46.8 34.8 all-gather.2
